TPU v7x, 32 devices: a whole 2x2x4 slice. The times are simulated.
32 devices in a mesh: ep: 16 (over z, y, x), tp: 2 (over core).
Axes of the slice: x: 2, y: 2, z: 4, core: 2. Of those that a mesh axis runs over, the one named last changes fastest.
Arguments:
- tokens: bfloat16 [512, 2048], P('ep'), may hold values from -6 to 6
- mix_gain: float32 [2048], replicated, may hold values from 0.1 to 1.9
- w_query: bfloat16 [2048, 512], P('ep', 'tp'), may hold values from -0.125 to 0.125
- w_key: bfloat16 [2048, 512], P('ep', 'tp'), may hold values from -0.125 to 0.125
- w_value: bfloat16 [2048, 512], P('ep', 'tp'), may hold values from -0.125 to 0.125
- w_outgate: bfloat16 [2048, 512], P('ep', 'tp'), may hold values from -0.125 to 0.125
- w_igate: bfloat16 [2048, 8], P('ep', 'tp'), may hold values from -0.125 to 0.125
- w_fgate: bfloat16 [2048, 8], P('ep', 'tp'), may hold values from -0.125 to 0.125
- igate_bias: float32 [8], P('tp'), may hold values from -2 to 1
- fgate_bias: float32 [8], P('tp'), may hold values from 0 to 4
- head_gain: float32 [512], P('tp'), may hold values from 0.1 to 1.9
- w_out: bfloat16 [512, 2048], P('tp', 'ep'), may hold values from -0.25 to 0.25
- state_matrix: float32 [512, 8, 64, 64], P('ep', 'tp'), may hold values from -2.4 to 2.4
- state_norm: float32 [512, 8, 64], P('ep', 'tp'), may hold values from -2.4 to 2.4
- state_max: float32 [512, 8], P('ep', 'tp'), may hold values from -4 to 4
- ffn_gain: float32 [2048], replicated, may hold values from 0.1 to 1.9
- w_expert_gate: bfloat16 [16, 2048, 1408], P('ep', None, 'tp'), may hold values from -0.125 to 0.125
- w_expert_up: bfloat16 [16, 2048, 1408], P('ep', None, 'tp'), may hold values from -0.125 to 0.125
- w_expert_down: bfloat16 [16, 1408, 2048], P('ep', 'tp'), may hold values from -0.15625 to 0.15625
- routes: int32 [512, 3], P('ep'), may hold values from 0 to 15, all different within a row; in each aligned block of 32 rows (0 to 31, 32 to 63, ...) at most 12 rows name the same one
- route_weights: float32 [512, 3], P('ep'), may hold values from 0.2 to 1
Outputs:
- mixed: bfloat16 [512, 2048], P('ep')
- new_matrix: float32 [512, 8, 64, 64], P('ep', 'tp')
- new_norm: float32 [512, 8, 64], P('ep', 'tp')
- new_max: float32 [512, 8], P('ep', 'tp')
Inputs may be any that keep to these rules, and one draw needn't show every extreme that they name: `routes`: each row names 3 different experts. Among the rows of one device, no expert is named by more than 12 rows, a bound that some block reaches.
All inputs are finite; a program needn't handle non-finite values.
Results may differ from a plain program's by a relative error of at most 0.017.
Values may be sent and summed in bfloat16 or wider, within the bound.
No kernel may reach another device: no remote copies, remote signals or barrier semaphores. Data moves between devices by JAX's collectives and lax.ppermute only.
A program may use at most 128 MiB of HBM per device.

v0:
```python
import jax
import jax.numpy as jnp
from jax import lax
from jax.sharding import PartitionSpec as P


def rms_scale(values_in, gain_vec):
    widened = values_in.astype(jnp.float32)
    return (
        widened * lax.rsqrt(jnp.mean(widened * widened, axis=-1, keepdims=True) + 1e-06) * gain_vec
    )


def memory_cell(
    query,
    key_row,
    value_row,
    outgate,
    input_pre,
    forget_pre,
    head_gain,
    state_matrix,
    state_norm,
    state_max,
):
    seq_rows, head_count = input_pre.shape
    head_size = query.shape[1] // head_count
    query_heads = query.astype(jnp.float32).reshape(seq_rows, head_count, head_size)
    key_heads = key_row.astype(jnp.float32).reshape(
        seq_rows, head_count, head_size
    ) * head_size ** (-0.5)
    value_heads = value_row.astype(jnp.float32).reshape(seq_rows, head_count, head_size)
    log_forget = jax.nn.log_sigmoid(forget_pre)
    new_max = jnp.maximum(log_forget + state_max, input_pre)
    keep_old = jnp.exp(log_forget + state_max - new_max)
    keep_new = jnp.exp(input_pre - new_max)
    new_matrix = (
        keep_old[:, :, None, None] * state_matrix
        + keep_new[:, :, None, None] * value_heads[:, :, :, None] * key_heads[:, :, None, :]
    )
    new_norm = keep_old[:, :, None] * state_norm + keep_new[:, :, None] * key_heads
    numerator = jnp.einsum(
        "bhvd,bhd->bhv", new_matrix, query_heads, precision=lax.Precision.HIGHEST
    )
    denominator = jnp.sum(new_norm * query_heads, axis=-1)
    cell_read = numerator / jnp.maximum(jnp.abs(denominator), jnp.exp(-new_max))[:, :, None]
    centered = cell_read - jnp.mean(cell_read, axis=-1, keepdims=True)
    variance = jnp.mean(centered * centered, axis=-1, keepdims=True)
    scaled_cell = (centered * lax.rsqrt(variance + 1e-06)).reshape(seq_rows, head_count * head_size)
    cell_out = (scaled_cell * head_gain * jax.nn.sigmoid(outgate.astype(jnp.float32))).astype(
        jnp.bfloat16
    )
    return (cell_out, new_matrix, new_norm, new_max)


def body(
    tokens,
    mix_gain,
    w_query,
    w_key,
    w_value,
    w_outgate,
    w_igate,
    w_fgate,
    igate_bias,
    fgate_bias,
    head_gain,
    w_out,
    state_matrix,
    state_norm,
    state_max,
    ffn_gain,
    w_expert_gate,
    w_expert_up,
    w_expert_down,
    routes,
    route_weights,
):
    seq_rows, width = tokens.shape
    normed = rms_scale(tokens, mix_gain).astype(jnp.bfloat16)
    weight_list = (w_query, w_key, w_value, w_outgate, w_igate, w_fgate)
    spread = lax.all_to_all(normed, "ep", split_axis=1, concat_axis=0, tiled=True)
    joined = jnp.concatenate(weight_list, axis=1)
    summed = lax.psum_scatter(
        jnp.dot(spread, joined, preferred_element_type=jnp.float32),
        "ep",
        scatter_dimension=0,
        tiled=True,
    )
    bounds = [0]
    for weight in weight_list:
        bounds.append(bounds[-1] + weight.shape[1])
    projected = tuple(
        (summed[:, bounds[index] : bounds[index + 1]] for index in range(len(weight_list)))
    )
    query = projected[0].astype(jnp.bfloat16)
    key_row = projected[1].astype(jnp.bfloat16)
    value_row = projected[2].astype(jnp.bfloat16)
    outgate = projected[3].astype(jnp.bfloat16)
    input_pre = projected[4] + igate_bias
    forget_pre = projected[5] + fgate_bias
    cell_out, new_matrix, new_norm, new_max = memory_cell(
        query,
        key_row,
        value_row,
        outgate,
        input_pre,
        forget_pre,
        head_gain,
        state_matrix,
        state_norm,
        state_max,
    )
    partial_out = jnp.dot(
        cell_out,
        lax.all_gather(w_out, "ep", axis=1, tiled=True),
        preferred_element_type=jnp.float32,
    )
    attended = lax.psum(partial_out.astype(jnp.bfloat16), "tp").astype(jnp.float32)
    resid = (tokens.astype(jnp.float32) + attended).astype(jnp.bfloat16)
    normed_two = rms_scale(resid, ffn_gain).astype(jnp.bfloat16)
    ep_count = lax.axis_size("ep")
    local_experts = w_expert_gate.shape[0]
    expert_total = local_experts * ep_count
    top_count = routes.shape[1]
    capacity = max(2, 2 * seq_rows * top_count // expert_total)
    flat_routes = routes.reshape(-1)
    onehot = (flat_routes[:, None] == jnp.arange(expert_total, dtype=jnp.int32)[None, :]).astype(
        jnp.int32
    )
    earlier = jnp.cumsum(onehot, axis=0, dtype=jnp.int32) - onehot
    slots = jnp.sum(onehot * earlier, axis=1, dtype=jnp.int32)
    targets = flat_routes * capacity + slots
    dispatch = (
        targets[:, None] == jnp.arange(expert_total * capacity, dtype=jnp.int32)[None, :]
    ).astype(jnp.bfloat16)
    route_rows = jnp.repeat(normed_two, top_count, axis=0)
    outgoing = jnp.einsum(
        "rs,rd->sd", dispatch, route_rows, preferred_element_type=jnp.float32
    ).astype(jnp.bfloat16)
    outgoing = outgoing.reshape(expert_total, capacity, width)
    received = lax.all_to_all(outgoing, "ep", split_axis=0, concat_axis=0, tiled=True)
    slot_count = received.shape[1]
    regrouped = received.reshape(ep_count, local_experts, slot_count, width)
    gate_pre = jnp.einsum(
        "nxcd,xdf->nxcf", regrouped, w_expert_gate, preferred_element_type=jnp.float32
    )
    up_pre = jnp.einsum(
        "nxcd,xdf->nxcf", regrouped, w_expert_up, preferred_element_type=jnp.float32
    )
    hidden = (jax.nn.silu(gate_pre) * up_pre).astype(jnp.bfloat16)
    partial_down = jnp.einsum(
        "nxcf,xfd->nxcd", hidden, w_expert_down, preferred_element_type=jnp.float32
    )
    expert_sum = lax.psum(partial_down.astype(jnp.bfloat16), "tp")
    finished = expert_sum.reshape(ep_count * local_experts, slot_count, width)
    returned = lax.all_to_all(finished, "ep", split_axis=0, concat_axis=0, tiled=True)
    picked = jnp.dot(
        dispatch,
        returned.reshape(expert_total * capacity, width),
        preferred_element_type=jnp.float32,
    )
    weighted = jnp.sum(
        picked.reshape(seq_rows, top_count, width) * route_weights[:, :, None], axis=1
    )
    mixed = (resid.astype(jnp.float32) + weighted).astype(jnp.bfloat16)
    return (mixed, new_matrix, new_norm, new_max)


def solution(mesh):
    placed = (
        P("ep", None),
        P(),
        P("ep", "tp"),
        P("ep", "tp"),
        P("ep", "tp"),
        P("ep", "tp"),
        P("ep", "tp"),
        P("ep", "tp"),
        P("tp"),
        P("tp"),
        P("tp"),
        P("tp", "ep"),
        P("ep", "tp", None, None),
        P("ep", "tp", None),
        P("ep", "tp"),
        P(),
        P("ep", None, "tp"),
        P("ep", None, "tp"),
        P("ep", "tp", None),
        P("ep", None),
        P("ep", None),
    )
    return jax.shard_map(
        body,
        mesh=mesh,
        in_specs=placed,
        out_specs=(P("ep", None), P("ep", "tp", None, None), P("ep", "tp", None), P("ep", "tp")),
        check_vma=False,
    )
```

profile of v0, /device:TPU:8, one launch (start us, length us, event | category | flops | bytes accessed | tf_op | source)
XLA Modules:
  0.0 342.0 jit_solution(8380659892496630698)
XLA Ops:
  7.2 1.2 fusion.36
  8.4 1.7 copy_bitcast_fusion
  10.1 7.2 %all-to-all-start = ((bf16[32,16,128]{2,0,1:T(8,128)(2,1)}), bf16[32,16,128]{2,0,1:T(8,128)(2,1)S(1)}, u32[]{:S(2)}, u32[]{:S(2)}) async-start(bf16[32,16,128]{2,0,1:T(8,128)(2,1)} %copy_bitcast_fusion), calls=%async_computation | async-start | bytes 262144 | tf_op jit(solution)/shard_map/all_to_all | solution.py:82
  17.3 0.8 copy.58
  18.1 0.8 copy.59
  19.0 1.1 concatenate.3
  20.0 3.9 %all-to-all-done = bf16[32,16,128]{2,0,1:T(8,128)(2,1)S(1)} async-done(((bf16[32,16,128]{2,0,1:T(8,128)(2,1)}), bf16[32,16,128]{2,0,1:T(8,128)(2,1)S(1)}, u32[]{:S(2)}, u32[]{:S(2)}) %all-to-all-start) | async-done | bytes 131104 | tf_op jit(solution)/shard_map/all_to_all | solution.py:82
  23.9 1.9 fusion.62
  25.8 0.7 all-gather.2.cloned.1.call-update
  26.8 0.1 eq.50
  27.0 0.1 reduce_window_sum.11
  27.1 0.2 select_reduce_fusion
  27.3 125.7 %reduce-scatter.2.cloned.1.call-done = f32[32,1032]{1,0:T(8,128)} async-done(((f32[512,1032]{1,0:T(8,128)}), f32[32,1032]{1,0:T(8,128)}) %reduce-scatter.2.cloned.1.call-update) | async-done | bytes 132112 | tf_op jit(solution)/shard_map/reduce_scatter | solution.py:84
  153.0 0.9 convert.9
  154.1 0.1 reshape.171
  154.4 0.9 broadcast_multiply_fusion.3
  155.3 0.8 subtract_exponential_fusion.1
  156.1 0.8 multiply_reduce_fusion.1
  156.9 3.8 %multiply_add_fusion = f32[32,4,64,64]{3,2,1,0:T(8,128)S(1)} fusion(f32[32,4,64,64]{3,2,1,0:T(8,128)} %param.33, f32[32,4,64]{2,1,0:T(4,128)S(1)} %get-tuple-element.30, f32[32,4,64]{2,1,0:T(4,128)S(1)} %get-tuple-element.31, f32[32,4]{1,0:T(8,128)S(1)} %subtract_exponential_fusion.1), kind=kLoop, calls=%fused_computation | loop fusion | flops 1572864 | bytes 4260352 | tf_op jit(solution)/shard_map/add | solution.py:38
  160.7 2.0 copy-done.1
  162.7 3.4 fusion.63
  166.1 0.2 fusion.59
  166.3 0.2 multiply_reduce_fusion
  166.5 0.1 subtract_multiply_fusion
  166.6 0.1 reshape.152
  166.7 39.0 %all-gather.2.cloned.1.call-done = bf16[256,2048]{1,0:T(8,128)(2,1)} async-done(((bf16[256,128]{1,0:T(8,128)(2,1)}), bf16[256,2048]{1,0:T(8,128)(2,1)}) %all-gather.2.cloned.1.call-update) | async-done | bytes 1048592 | tf_op jit(solution)/shard_map/all_gather | solution.py:116
  205.7 2.2 convolution_convert_fusion.1
  207.9 0.5 multiply_add_fusion.3
  208.4 18.1 %all-reduce.3.cloned.1.call-done = bf16[32,2048]{1,0:T(8,128)(2,1)} async-done(((bf16[32,2048]{1,0:T(8,128)(2,1)}), bf16[32,2048]{1,0:T(8,128)(2,1)}) %all-reduce.3.cloned.1.call-update) | async-done | bytes 131088 | tf_op jit(solution)/shard_map/psum | solution.py:119
  226.5 1.1 fusion.40
  227.6 1.0 fusion.42
  228.6 0.2 broadcast_in_dim.2
  228.8 1.1 reshape.153
  229.9 2.4 convolution_convert_fusion
  232.3 2.1 reshape.154
  234.4 33.1 %all_to_all.29 = bf16[16,12,2048]{2,1,0:T(8,128)(2,1)S(1)} all-to-all(bf16[16,12,2048]{2,1,0:T(8,128)(2,1)} %reshape.154), channel_id=1, replica_groups=mesh['ep'=16,'tp'=2] {'ep'}, dimensions={0} | all-to-all | bytes 1572864 | tf_op jit(solution)/shard_map/all_to_all | solution.py:142
  267.5 1.0 copy-done.4
  268.5 3.8 %fusion.9 = f32[16,1,12,704]{3,0,2,1:T(8,128)} fusion(bf16[1,2048,704]{1,2,0:T(8,128)(2,1)} %param.37, bf16[16,12,2048]{2,1,0:T(8,128)(2,1)S(1)} %all_to_all.29), kind=kOutput, calls=%fused_computation.11 | convolution fusion | flops 553648128 | bytes 4210688 | tf_op jit(solution)/shard_map/nxcd,xdf->nxcf/dot_general | solution.py:145
  272.3 5.2 %fusion.6 = bf16[16,12,2048]{2,0,1:T(8,128)(2,1)} fusion(bf16[1,704,2048]{2,1,0:T(8,128)(2,1)S(1)} %copy-done, bf16[1,2048,704]{1,2,0:T(8,128)(2,1)} %param.38, f32[16,1,12,704]{3,0,2,1:T(8,128)} %fusion.9, bf16[16,12,2048]{2,1,0:T(8,128)(2,1)} %copy-done.4), kind=kOutput, calls=%fused_computation.7 | convolution fusion | flops 1108500480 | bytes 7880704 | tf_op jit(solution)/shard_map/nxcf,xfd->nxcd/dot_general | solution.py:152
  277.6 17.9 %all-reduce.5.cloned.1.call-done = bf16[16,12,2048]{2,0,1:T(8,128)(2,1)} async-done(((bf16[16,12,2048]{2,0,1:T(8,128)(2,1)}), bf16[16,12,2048]{2,0,1:T(8,128)(2,1)}) %all-reduce.5.cloned.1.call-update) | async-done | bytes 786448 | tf_op jit(solution)/shard_map/psum | solution.py:155
  295.5 2.6 copy.65
  298.1 7.1 %all-to-all-start.2 = ((bf16[16,12,2048]{2,1,0:T(8,128)(2,1)}), bf16[16,12,2048]{2,1,0:T(8,128)(2,1)}, u32[]{:S(2)}, u32[]{:S(2)}) async-start(bf16[16,12,2048]{2,1,0:T(8,128)(2,1)} %copy.65), calls=%async_computation.3 | async-start | bytes 2097152 | tf_op jit(solution)/shard_map/all_to_all | solution.py:157
  305.2 0.1 reduce_sum.70
  305.4 0.7 copy.66
  306.0 25.1 %all-to-all-done.2 = bf16[16,12,2048]{2,1,0:T(8,128)(2,1)} async-done(((bf16[16,12,2048]{2,1,0:T(8,128)(2,1)}), bf16[16,12,2048]{2,1,0:T(8,128)(2,1)}, u32[]{:S(2)}, u32[]{:S(2)}) %all-to-all-start.2) | async-done | bytes 786464 | tf_op jit(solution)/shard_map/all_to_all | solution.py:157
  331.1 2.1 reshape.169
  333.2 1.5 fusion.18
  334.7 0.7 fusion.43
  (51 shorter events, 0.9 us)
Async XLA Ops:
  7.2 265.2 %copy-start = (bf16[1,704,2048]{2,1,0:T(8,128)(2,1)S(1)}, bf16[1,704,2048]{2,1,0:T(8,128)(2,1)}, u32[]{:S(2)}) copy-start(bf16[1,704,2048]{2,1,0:T(8,128)(2,1)} %param.39) | copy-start | bytes 8650756
  10.1 13.8 %all-to-all-start = ((bf16[32,16,128]{2,0,1:T(8,128)(2,1)}), bf16[32,16,128]{2,0,1:T(8,128)(2,1)S(1)}, u32[]{:S(2)}, u32[]{:S(2)}) async-start(bf16[32,16,128]{2,0,1:T(8,128)(2,1)} %copy_bitcast_fusion), calls=%async_computation | async-start | bytes 262144 | tf_op jit(solution)/shard_map/all_to_all | solution.py:82
  17.3 135.7 %reduce-scatter.2.cloned.1.call-start = ((), (), s32[]{:S(2)}) async-start(), calls=%async_computation.4 | async-start | bytes 2506752 | tf_op jit(solution)/shard_map/reduce_scatter | solution.py:84
  18.9 7.6 %copy-start.13 = (f32[32,4]{0,1:T(4,128)S(1)}, f32[32,4]{0,1:T(4,128)}, u32[]{:S(2)}) copy-start(f32[32,4]{0,1:T(4,128)} %param.35) | copy-start | bytes 1540
  18.9 7.7 %copy-start.7 = (s32[32,3]{0,1:T(4,128)S(1)}, s32[32,3]{0,1:T(4,128)}, u32[]{:S(2)}) copy-start(s32[32,3]{0,1:T(4,128)} %param.40) | copy-start | bytes 1156
  23.9 130.5 %copy-start.10 = (f32[4]{0:T(128)S(1)}, f32[4]{0:T(128)}, u32[]{:S(2)}) copy-start(f32[4]{0:T(128)} %param.30) | copy-start | bytes 52
  23.9 130.5 %copy-start.15 = (f32[4]{0:T(128)S(1)}, f32[4]{0:T(128)}, u32[]{:S(2)}) copy-start(f32[4]{0:T(128)} %param.29) | copy-start | bytes 52
  23.9 132.2 %copy-start.5 = (f32[32,4,64]{2,1,0:T(4,128)S(1)}, f32[32,4,64]{2,1,0:T(4,128)}, u32[]{:S(2)}) copy-start(f32[32,4,64]{2,1,0:T(4,128)} %param.34) | copy-start | bytes 98308
  25.8 179.9 %all-gather.2.cloned.1.call-start = ((), (), s32[]{:S(2)}) async-start(), calls=%async_computation.5 | async-start | bytes 1114112 | tf_op jit(solution)/shard_map/all_gather | solution.py:116
  26.5 200.0 %all-reduce.3.cloned.1.call-start = ((), (), s32[]{:S(2)}) async-start(), calls=%async_computation.6 | async-start | bytes 262144 | tf_op jit(solution)/shard_map/psum | solution.py:119
  27.3 180.6 %copy-start.11 = (s32[96]{0:T(128)}, s32[96]{0:T(128)S(1)}, u32[]{:S(2)}) copy-start(s32[96]{0:T(128)S(1)} %select_reduce_fusion) | copy-start | bytes 1156
  160.7 2.0 copy-start.1
  162.7 43.0 %copy-start.14 = (f32[256]{0:T(256)S(1)}, f32[256]{0:T(256)}, u32[]{:S(2)}) copy-start(f32[256]{0:T(256)} %param.31) | copy-start | bytes 3076
  162.7 63.8 %copy-start.2 = (bf16[32,2048]{1,0:T(8,128)(2,1)S(1)}, bf16[32,2048]{1,0:T(8,128)(2,1)}, u32[]{:S(2)}) copy-start(bf16[32,2048]{1,0:T(8,128)(2,1)} %param.21) | copy-start | bytes 393220
  162.7 64.9 %copy-start.6 = (f32[2048]{0:T(1024)S(1)}, f32[2048]{0:T(1024)}, u32[]{:S(2)}) copy-start(f32[2048]{0:T(1024)} %param.36) | copy-start | bytes 24580
  207.9 87.6 %all-reduce.5.cloned.1.call-start = ((), (), s32[]{:S(2)}) async-start(), calls=%async_computation.7 | async-start | bytes 1572864 | tf_op jit(solution)/shard_map/psum | solution.py:155
  267.5 1.0 copy-start.4
  277.5 27.7 %copy-start.12 = (s32[96]{0:T(128)S(1)}, s32[96]{0:T(128)}, u32[]{:S(2)}) copy-start(s32[96]{0:T(128)} %copy-done.11) | copy-start | bytes 1156
  277.5 27.8 %copy-start.8 = (s32[32,3]{0,1:T(4,128)S(1)}, s32[32,3]{0,1:T(4,128)}, u32[]{:S(2)}) copy-start(s32[32,3]{0,1:T(4,128)} %param.40) | copy-start | bytes 1156
  277.6 55.7 %copy-start.9 = (f32[32,3]{0,1:T(4,128)S(1)}, f32[32,3]{0,1:T(4,128)}, u32[]{:S(2)}) copy-start(f32[32,3]{0,1:T(4,128)} %param.41) | copy-start | bytes 1156
  298.1 36.6 %copy-start.3 = (bf16[32,2048]{1,0:T(8,128)(2,1)S(1)}, bf16[32,2048]{1,0:T(8,128)(2,1)}, u32[]{:S(2)}) copy-start(bf16[32,2048]{1,0:T(8,128)(2,1)} %all-reduce.3.cloned.1.call-done) | copy-start | bytes 393220
  298.1 33.0 %all-to-all-start.2 = ((bf16[16,12,2048]{2,1,0:T(8,128)(2,1)}), bf16[16,12,2048]{2,1,0:T(8,128)(2,1)}, u32[]{:S(2)}, u32[]{:S(2)}) async-start(bf16[16,12,2048]{2,1,0:T(8,128)(2,1)} %copy.65), calls=%async_computation.3 | async-start | bytes 2097152 | tf_op jit(solution)/shard_map/all_to_all | solution.py:157
Sparse Core Ops, SparseCore 0:
  25.9 127.0 reduce-scatter.1
  155.7 49.9 all-gather.1
  208.6 17.9 all-reduce.2
  277.7 17.7 all-reduce.4
where the time goes:
time: 343 us; the launch traced here: 342 us
  waiting for transfers between devices  230 us (67%)
  blocking collectives  33.1 us (10%)
  matrix products  20.2 us (6%)
  local copies, waits for them, and re-layouts  15.4 us (4%)
  starting transfers between devices  14.5 us (4%)
  other arithmetic  14.3 us (4%)
  between operations  14 us (4%)
    reduce_scatter x1, waiting for transfers between devices, body(): lax.psum_scatter(jnp.dot(spread, joined, preferred_element_type=jnp.float...  126 us
    all_gather x1, waiting for transfers between devices, body(): lax.all_gather(w_out, 'ep', axis=1, tiled=True)  39 us
    all_to_all x1, blocking collectives, body(): lax.all_to_all(outgoing, 'ep', split_axis=0, concat_axis=0, tiled=True)  33.1 us
    all_to_all x1, waiting for transfers between devices, body(): lax.all_to_all(finished, 'ep', split_axis=0, concat_axis=0, tiled=True)  25.1 us
    psum x1, waiting for transfers between devices, body(): lax.psum(partial_out.astype(jnp.bfloat16), 'tp').astype(jnp.float32)  18.1 us
    psum x1, waiting for transfers between devices, body(): expert_sum = lax.psum(partial_down.astype(jnp.bfloat16), 'tp')  17.9 us
    all_to_all x1, starting transfers between devices, body(): lax.all_to_all(normed, 'ep', split_axis=1, concat_axis=0, tiled=True)  7.22 us
    all_to_all x1, starting transfers between devices, body(): lax.all_to_all(finished, 'ep', split_axis=0, concat_axis=0, tiled=True)  7.11 us
  transfers between devices with their start and end apart: 6, of which 6 were waited for; matrix products, arithmetic and copies ran while one was open for 5% of the time, Pallas kernels for 0%

commit v1 on v0

--- a/solution.py
+++ b/solution.py
@@ -2,6 +2,18 @@
 import jax.numpy as jnp
 from jax import lax
 from jax.sharding import PartitionSpec as P
+from jax.lax import axis_index, axis_size, ppermute
+
+
+def do_works_now(q_in, pos_dim, view):
+    latest, all_rows = (q_in.shape[:pos_dim], q_in.shape[pos_dim + 1 :])
+    return jnp.moveaxis(q_in.reshape(*latest, view, -1, *all_rows), pos_dim, 0)
+
+
+def carry_the_sides(own_rows, ndim_at):
+    arr_out = list(own_rows.shape[1:])
+    arr_out[ndim_at] *= own_rows.shape[0]
+    return jnp.moveaxis(own_rows, 0, ndim_at).reshape(arr_out)
 
 
 def rms_scale(values_in, gain_vec):
@@ -139,7 +151,20 @@
         "rs,rd->sd", dispatch, route_rows, preferred_element_type=jnp.float32
     ).astype(jnp.bfloat16)
     outgoing = outgoing.reshape(expert_total, capacity, width)
-    received = lax.all_to_all(outgoing, "ep", split_axis=0, concat_axis=0, tiled=True)
+    arr_now, piece_now = (axis_size("ep"), axis_index("ep"))
+    outcome_arr = do_works_now(outgoing, 0, arr_now)
+    shelf = [outcome_arr[piece_now]]
+    nth = 1
+    while nth < arr_now:
+        next_value = outcome_arr[(piece_now + nth) % arr_now]
+        shelf.append(
+            ppermute(
+                next_value, axis_name="ep", perm=[(t, (t + nth) % arr_now) for t in range(arr_now)]
+            )
+        )
+        nth = nth + 1
+    outcome_arr = jnp.stack(shelf)[(piece_now - jnp.arange(arr_now)) % arr_now]
+    received = carry_the_sides(outcome_arr, 0)
     slot_count = received.shape[1]
     regrouped = received.reshape(ep_count, local_experts, slot_count, width)
     gate_pre = jnp.einsum(

time: 343 us -> 391 us (1.14)
  waiting for transfers between devices: 230 us -> 268 us
  blocking collectives: 33.1 us -> 0 us
  starting transfers between devices: 14.5 us -> 44.2 us
  local copies, waits for them, and re-layouts: 15.4 us -> 28.6 us
    ppermute x0 -> x15, waiting for transfers between devices: none -> 33.5 us  [body(): ppermute(next_value, axis_name='ep', perm=[(t, (t + nth) % arr_now) for t...]
    all_to_all x1 -> x0, blocking collectives: 33.1 us -> none  [body(): lax.all_to_all(outgoing, 'ep', split_axis=0, concat_axis=0, tiled=True)]
    ppermute x0 -> x15, starting transfers between devices: none -> 29.7 us  [body(): ppermute(next_value, axis_name='ep', perm=[(t, (t + nth) % arr_now) for t...]
    unnamed x37 -> x51, local copies, waits for them, and re-layouts: 5.5 us -> 13.3 us
    psum x1, waiting for transfers between devices: 17.9 us -> 22.6 us  [body(): expert_sum = lax.psum(partial_down.astype(jnp.bfloat16), 'tp')]
  transfers between devices with their start and end apart: 6 -> 21, of which waited for: 6 -> 16; matrix products, arithmetic and copies ran while one was open for 5% -> 7% of each run, Pallas kernels for 0% -> 0%
where the time goes in v1:
time: 391 us; the launch traced here: 390 us
  waiting for transfers between devices  268 us (69%)
  starting transfers between devices  44.2 us (11%)
  local copies, waits for them, and re-layouts  28.6 us (7%)
  matrix products  20.5 us (5%)
  other arithmetic  14.8 us (4%)
  between operations  14 us (4%)
    reduce_scatter x1, waiting for transfers between devices, body(): lax.psum_scatter(jnp.dot(spread, joined, preferred_element_type=jnp.float...  126 us
    all_gather x1, waiting for transfers between devices, body(): lax.all_gather(w_out, 'ep', axis=1, tiled=True)  39 us
    ppermute x15, waiting for transfers between devices, body(): ppermute(next_value, axis_name='ep', perm=[(t, (t + nth) % arr_now) for t...  33.5 us
    ppermute x15, starting transfers between devices, body(): ppermute(next_value, axis_name='ep', perm=[(t, (t + nth) % arr_now) for t...  29.7 us
    all_to_all x1, waiting for transfers between devices, body(): lax.all_to_all(finished, 'ep', split_axis=0, concat_axis=0, tiled=True)  25.1 us
    psum x1, waiting for transfers between devices, body(): expert_sum = lax.psum(partial_down.astype(jnp.bfloat16), 'tp')  22.6 us
    psum x1, waiting for transfers between devices, body(): lax.psum(partial_out.astype(jnp.bfloat16), 'tp').astype(jnp.float32)  17.5 us
    unnamed x51, local copies, waits for them, and re-layouts  13.3 us
  transfers between devices with their start and end apart: 21, of which 16 were waited for; matrix products, arithmetic and copies ran while one was open for 7% of the time, Pallas kernels for 0%

profile of v1, /device:TPU:8, one launch (start us, length us, event | category | flops | bytes accessed | tf_op | source)
XLA Modules:
  0.0 390.3 jit_solution(4836763113091637783)
XLA Ops:
  7.2 1.2 fusion.36
  8.4 1.7 copy_bitcast_fusion
  10.1 7.2 %all-to-all-start = ((bf16[32,16,128]{2,0,1:T(8,128)(2,1)}), bf16[32,16,128]{2,0,1:T(8,128)(2,1)S(1)}, u32[]{:S(2)}, u32[]{:S(2)}) async-start(bf16[32,16,128]{2,0,1:T(8,128)(2,1)} %copy_bitcast_fusion), calls=%async_computation | async-start | bytes 262144 | tf_op jit(solution)/shard_map/all_to_all | solution.py:94
  19.0 1.1 concatenate.3
  20.0 3.9 all-to-all-done
  23.9 1.9 fusion.64
  27.3 125.8 %reduce-scatter.2.cloned.1.call-done = f32[32,1032]{1,0:T(8,128)} async-done(((f32[512,1032]{1,0:T(8,128)}), f32[32,1032]{1,0:T(8,128)}) %reduce-scatter.2.cloned.1.call-update) | async-done | bytes 132112 | tf_op jit(solution)/shard_map/reduce_scatter | solution.py:96
  157.0 3.7 multiply_add_fusion
  160.7 2.0 copy-done.1
  162.7 3.4 fusion.65
  166.7 39.0 %all-gather.2.cloned.1.call-done = bf16[256,2048]{1,0:T(8,128)(2,1)} async-done(((bf16[256,128]{1,0:T(8,128)(2,1)}), bf16[256,2048]{1,0:T(8,128)(2,1)}) %all-gather.2.cloned.1.call-update) | async-done | bytes 1048592 | tf_op jit(solution)/shard_map/all_gather | solution.py:128
  205.7 2.2 convolution_convert_fusion.1
  209.1 17.5 %all-reduce.3.cloned.1.call-done = bf16[32,2048]{1,0:T(8,128)(2,1)} async-done(((bf16[32,2048]{1,0:T(8,128)(2,1)}), bf16[32,2048]{1,0:T(8,128)(2,1)}) %all-reduce.3.cloned.1.call-update) | async-done | bytes 131088 | tf_op jit(solution)/shard_map/psum | solution.py:131
  226.6 1.1 fusion.40
  227.7 1.0 fusion.42
  228.9 1.1 reshape.198
  230.0 2.4 convolution_convert_fusion
  232.4 2.1 reshape_reshape.3
  234.5 2.0 dynamic-slice_bitcast_fusion
  236.5 1.5 collective-permute-start
  238.0 2.4 collective-permute-start.14
  240.9 3.3 collective-permute-start.12
  246.0 4.0 %collective-permute-done.1 = bf16[1,12,2048]{2,1,0:T(8,128)(2,1)S(1)} collective-permute-done((bf16[1,12,2048]{2,1,0:T(8,128)(2,1)S(1)}, bf16[1,12,2048]{2,1,0:T(8,128)(2,1)S(1)}, u32[]{:S(2)}, u32[]{:S(2)}) %collective-permute-start.1) | collective-permute-done | bytes 49184 | tf_op jit(solution)/shard_map/ppermute | solution.py:161
  250.0 1.5 collective-permute-start.2
  252.1 4.3 %collective-permute-done.2 = bf16[1,12,2048]{2,1,0:T(8,128)(2,1)S(1)} collective-permute-done((bf16[1,12,2048]{2,1,0:T(8,128)(2,1)S(1)}, bf16[1,12,2048]{2,1,0:T(8,128)(2,1)S(1)}, u32[]{:S(2)}, u32[]{:S(2)}) %collective-permute-start.2) | collective-permute-done | bytes 49184 | tf_op jit(solution)/shard_map/ppermute | solution.py:161
  257.3 4.3 %collective-permute-done.3 = bf16[1,12,2048]{2,1,0:T(8,128)(2,1)S(1)} collective-permute-done((bf16[1,12,2048]{2,1,0:T(8,128)(2,1)S(1)}, bf16[1,12,2048]{2,1,0:T(8,128)(2,1)S(1)}, u32[]{:S(2)}, u32[]{:S(2)}) %collective-permute-start.3) | collective-permute-done | bytes 49184 | tf_op jit(solution)/shard_map/ppermute | solution.py:161
  262.9 6.0 %collective-permute-done.4 = bf16[1,12,2048]{2,1,0:T(8,128)(2,1)S(1)} collective-permute-done((bf16[1,12,2048]{2,1,0:T(8,128)(2,1)S(1)}, bf16[1,12,2048]{2,1,0:T(8,128)(2,1)S(1)}, u32[]{:S(2)}, u32[]{:S(2)}) %collective-permute-start.4) | collective-permute-done | bytes 49184 | tf_op jit(solution)/shard_map/ppermute | solution.py:161
  269.0 1.0 collective-permute-start.5
  270.6 4.5 %collective-permute-done.5 = bf16[1,12,2048]{2,1,0:T(8,128)(2,1)S(1)} collective-permute-done((bf16[1,12,2048]{2,1,0:T(8,128)(2,1)S(1)}, bf16[1,12,2048]{2,1,0:T(8,128)(2,1)S(1)}, u32[]{:S(2)}, u32[]{:S(2)}) %collective-permute-start.5) | collective-permute-done | bytes 49184 | tf_op jit(solution)/shard_map/ppermute | solution.py:161
  275.1 4.2 %collective-permute-start.6 = (bf16[1,12,2048]{2,1,0:T(8,128)(2,1)S(1)}, bf16[1,12,2048]{2,1,0:T(8,128)(2,1)S(1)}, u32[]{:S(2)}, u32[]{:S(2)}) collective-permute-start(bf16[1,12,2048]{2,1,0:T(8,128)(2,1)S(1)} %get-tuple-element.35), channel_id=1, source_target_pairs={{0,14},{2,16},{4,18},{6,20},{8,22},{10,24},{12,26},{14,28},{16,30}... | collective-permute-start | bytes 147464 | tf_op jit(solution)/shard_map/ppermute | solution.py:161
  279.9 1.3 collective-permute-done.6
  281.2 3.9 %collective-permute-start.7 = (bf16[1,12,2048]{2,1,0:T(8,128)(2,1)S(1)}, bf16[1,12,2048]{2,1,0:T(8,128)(2,1)S(1)}, u32[]{:S(2)}, u32[]{:S(2)}) collective-permute-start(bf16[1,12,2048]{2,1,0:T(8,128)(2,1)S(1)} %get-tuple-element.34), channel_id=1, source_target_pairs={{0,16},{2,18},{4,20},{6,22},{8,24},{10,26},{12,28},{14,30},{16,0},... | collective-permute-start | bytes 147464 | tf_op jit(solution)/shard_map/ppermute | solution.py:161
  285.7 1.6 collective-permute-done.7
  287.4 3.7 collective-permute-start.8
  291.7 1.8 collective-permute-done.8
  293.4 3.4 collective-permute-start.9
  297.5 3.3 collective-permute-done.9
  300.8 2.0 collective-permute-start.10
  303.5 2.5 collective-permute-done.10
  309.1 2.8 gather_fusion
  311.9 4.1 %fusion.9 = f32[16,1,12,704]{3,0,2,1:T(8,128)} fusion(bf16[1,2048,704]{1,2,0:T(8,128)(2,1)} %param.37, bf16[16,12,2048]{2,1,0:T(8,128)(2,1)} %gather_fusion), kind=kOutput, calls=%fused_computation.12 | convolution fusion | flops 553648128 | bytes 4210688 | tf_op jit(solution)/shard_map/nxcd,xdf->nxcf/dot_general | solution.py:170
  316.0 5.2 %fusion.6 = bf16[16,12,2048]{2,0,1:T(8,128)(2,1)} fusion(bf16[1,704,2048]{2,1,0:T(8,128)(2,1)S(1)} %copy-done, bf16[1,2048,704]{1,2,0:T(8,128)(2,1)} %param.38, f32[16,1,12,704]{3,0,2,1:T(8,128)} %fusion.9, bf16[16,12,2048]{2,1,0:T(8,128)(2,1)} %gather_fusion), kind=kOutput, calls=%fused_computation.8 | convolution fusion | flops 1108500480 | bytes 7880704 | tf_op jit(solution)/shard_map/nxcf,xfd->nxcd/dot_general | solution.py:177
  321.2 22.6 %all-reduce.5.cloned.1.call-done = bf16[16,12,2048]{2,0,1:T(8,128)(2,1)} async-done(((bf16[16,12,2048]{2,0,1:T(8,128)(2,1)}), bf16[16,12,2048]{2,0,1:T(8,128)(2,1)}) %all-reduce.5.cloned.1.call-update) | async-done | bytes 786448 | tf_op jit(solution)/shard_map/psum | solution.py:180
  343.8 2.6 copy.65
  346.4 7.1 %all-to-all-start.1 = ((bf16[16,12,2048]{2,1,0:T(8,128)(2,1)}), bf16[16,12,2048]{2,1,0:T(8,128)(2,1)}, u32[]{:S(2)}, u32[]{:S(2)}) async-start(bf16[16,12,2048]{2,1,0:T(8,128)(2,1)} %copy.65), calls=%async_computation.2 | async-start | bytes 2097152 | tf_op jit(solution)/shard_map/all_to_all | solution.py:182
  354.4 25.1 %all-to-all-done.1 = bf16[16,12,2048]{2,1,0:T(8,128)(2,1)} async-done(((bf16[16,12,2048]{2,1,0:T(8,128)(2,1)}), bf16[16,12,2048]{2,1,0:T(8,128)(2,1)}, u32[]{:S(2)}, u32[]{:S(2)}) %all-to-all-start.1) | async-done | bytes 786464 | tf_op jit(solution)/shard_map/all_to_all | solution.py:182
  379.4 2.1 reshape.225
  381.6 1.5 fusion.18
  (99 shorter events, 22.7 us)
Async XLA Ops:
  7.2 308.9 %copy-start = (bf16[1,704,2048]{2,1,0:T(8,128)(2,1)S(1)}, bf16[1,704,2048]{2,1,0:T(8,128)(2,1)}, u32[]{:S(2)}) copy-start(bf16[1,704,2048]{2,1,0:T(8,128)(2,1)} %param.39) | copy-start | bytes 8650756
  10.1 13.8 %all-to-all-start = ((bf16[32,16,128]{2,0,1:T(8,128)(2,1)}), bf16[32,16,128]{2,0,1:T(8,128)(2,1)S(1)}, u32[]{:S(2)}, u32[]{:S(2)}) async-start(bf16[32,16,128]{2,0,1:T(8,128)(2,1)} %copy_bitcast_fusion), calls=%async_computation | async-start | bytes 262144 | tf_op jit(solution)/shard_map/all_to_all | solution.py:94
  17.3 135.8 %reduce-scatter.2.cloned.1.call-start = ((), (), s32[]{:S(2)}) async-start(), calls=%async_computation.3 | async-start | bytes 2506752 | tf_op jit(solution)/shard_map/reduce_scatter | solution.py:96
  18.9 7.6 %copy-start.12 = (f32[32,4]{0,1:T(4,128)S(1)}, f32[32,4]{0,1:T(4,128)}, u32[]{:S(2)}) copy-start(f32[32,4]{0,1:T(4,128)} %param.35) | copy-start | bytes 1540
  18.9 7.7 %copy-start.6 = (s32[32,3]{0,1:T(4,128)S(1)}, s32[32,3]{0,1:T(4,128)}, u32[]{:S(2)}) copy-start(s32[32,3]{0,1:T(4,128)} %param.40) | copy-start | bytes 1156
  23.9 130.5 %copy-start.9 = (f32[4]{0:T(128)S(1)}, f32[4]{0:T(128)}, u32[]{:S(2)}) copy-start(f32[4]{0:T(128)} %param.30) | copy-start | bytes 52
  23.9 130.5 %copy-start.14 = (f32[4]{0:T(128)S(1)}, f32[4]{0:T(128)}, u32[]{:S(2)}) copy-start(f32[4]{0:T(128)} %param.29) | copy-start | bytes 52
  23.9 132.3 %copy-start.4 = (f32[32,4,64]{2,1,0:T(4,128)S(1)}, f32[32,4,64]{2,1,0:T(4,128)}, u32[]{:S(2)}) copy-start(f32[32,4,64]{2,1,0:T(4,128)} %param.34) | copy-start | bytes 98308
  25.8 180.0 %all-gather.2.cloned.1.call-start = ((), (), s32[]{:S(2)}) async-start(), calls=%async_computation.4 | async-start | bytes 1114112 | tf_op jit(solution)/shard_map/all_gather | solution.py:128
  26.5 200.1 %all-reduce.3.cloned.1.call-start = ((), (), s32[]{:S(2)}) async-start(), calls=%async_computation.5 | async-start | bytes 262144 | tf_op jit(solution)/shard_map/psum | solution.py:131
  27.3 180.7 %copy-start.10 = (s32[96]{0:T(128)}, s32[96]{0:T(128)S(1)}, u32[]{:S(2)}) copy-start(s32[96]{0:T(128)S(1)} %select_reduce_fusion) | copy-start | bytes 1156
  160.7 2.0 copy-start.1
  162.7 43.0 %copy-start.13 = (f32[256]{0:T(256)S(1)}, f32[256]{0:T(256)}, u32[]{:S(2)}) copy-start(f32[256]{0:T(256)} %param.31) | copy-start | bytes 3076
  162.7 63.9 %copy-start.2 = (bf16[32,2048]{1,0:T(8,128)(2,1)S(1)}, bf16[32,2048]{1,0:T(8,128)(2,1)}, u32[]{:S(2)}) copy-start(bf16[32,2048]{1,0:T(8,128)(2,1)} %param.21) | copy-start | bytes 393220
  162.7 64.9 %copy-start.5 = (f32[2048]{0:T(1024)S(1)}, f32[2048]{0:T(1024)}, u32[]{:S(2)}) copy-start(f32[2048]{0:T(1024)} %param.36) | copy-start | bytes 24580
  207.9 135.9 %all-reduce.5.cloned.1.call-start = ((), (), s32[]{:S(2)}) async-start(), calls=%async_computation.6 | async-start | bytes 1572864 | tf_op jit(solution)/shard_map/psum | solution.py:180
  230.0 8.0 %copy-start.15 = (s32[16]{0:T(128)S(1)}, s32[16]{0:T(128)}, u32[]{:S(2)}) copy-start(s32[16]{0:T(128)} %fusion.58) | copy-start | bytes 196
  236.5 8.3 %collective-permute-start = (bf16[1,12,2048]{2,1,0:T(8,128)(2,1)S(1)}, bf16[1,12,2048]{2,1,0:T(8,128)(2,1)S(1)}, u32[]{:S(2)}, u32[]{:S(2)}) collective-permute-start(bf16[1,12,2048]{2,1,0:T(8,128)(2,1)S(1)} %get-tuple-element.41), channel_id=1, source_target_pairs={{0,2},{2,4},{4,6},{6,8},{8,10},{10,12},{12,14},{14,16},{16,18},{18... | collective-permute-start | bytes 147464 | tf_op jit(solution)/shard_map/ppermute | solution.py:161
  238.0 70.5 %collective-permute-start.14 = (bf16[1,12,2048]{2,1,0:T(8,128)(2,1)S(1)}, bf16[1,12,2048]{2,1,0:T(8,128)(2,1)S(1)}, u32[]{:S(2)}, u32[]{:S(2)}) collective-permute-start(bf16[1,12,2048]{2,1,0:T(8,128)(2,1)S(1)} %get-tuple-element.27), channel_id=1, source_target_pairs={{0,30},{2,0},{4,2},{6,4},{8,6},{10,8},{12,10},{14,12},{16,14},{18,... | collective-permute-start | bytes 147464 | tf_op jit(solution)/shard_map/ppermute | solution.py:161
  240.4 67.5 %collective-permute-start.13 = (bf16[1,12,2048]{2,1,0:T(8,128)(2,1)S(1)}, bf16[1,12,2048]{2,1,0:T(8,128)(2,1)S(1)}, u32[]{:S(2)}, u32[]{:S(2)}) collective-permute-start(bf16[1,12,2048]{2,1,0:T(8,128)(2,1)S(1)} %get-tuple-element.28), channel_id=1, source_target_pairs={{0,28},{2,30},{4,0},{6,2},{8,4},{10,6},{12,8},{14,10},{16,12},{18,... | collective-permute-start | bytes 147464 | tf_op jit(solution)/shard_map/ppermute | solution.py:161
  240.9 66.3 %collective-permute-start.12 = (bf16[1,12,2048]{2,1,0:T(8,128)(2,1)S(1)}, bf16[1,12,2048]{2,1,0:T(8,128)(2,1)S(1)}, u32[]{:S(2)}, u32[]{:S(2)}) collective-permute-start(bf16[1,12,2048]{2,1,0:T(8,128)(2,1)S(1)} %get-tuple-element.29), channel_id=1, source_target_pairs={{0,26},{2,28},{4,30},{6,0},{8,2},{10,4},{12,6},{14,8},{16,10},{18,... | collective-permute-start | bytes 147464 | tf_op jit(solution)/shard_map/ppermute | solution.py:161
  244.3 62.3 %collective-permute-start.11 = (bf16[1,12,2048]{2,1,0:T(8,128)(2,1)S(1)}, bf16[1,12,2048]{2,1,0:T(8,128)(2,1)S(1)}, u32[]{:S(2)}, u32[]{:S(2)}) collective-permute-start(bf16[1,12,2048]{2,1,0:T(8,128)(2,1)S(1)} %get-tuple-element.30), channel_id=1, source_target_pairs={{0,24},{2,26},{4,28},{6,30},{8,0},{10,2},{12,4},{14,6},{16,8},{18,... | collective-permute-start | bytes 147464 | tf_op jit(solution)/shard_map/ppermute | solution.py:161
  244.8 5.2 %collective-permute-start.1 = (bf16[1,12,2048]{2,1,0:T(8,128)(2,1)S(1)}, bf16[1,12,2048]{2,1,0:T(8,128)(2,1)S(1)}, u32[]{:S(2)}, u32[]{:S(2)}) collective-permute-start(bf16[1,12,2048]{2,1,0:T(8,128)(2,1)S(1)} %get-tuple-element.40), channel_id=1, source_target_pairs={{0,4},{2,6},{4,8},{6,10},{8,12},{10,14},{12,16},{14,18},{16,20},{1... | collective-permute-start | bytes 147464 | tf_op jit(solution)/shard_map/ppermute | solution.py:161
  250.0 6.4 %collective-permute-start.2 = (bf16[1,12,2048]{2,1,0:T(8,128)(2,1)S(1)}, bf16[1,12,2048]{2,1,0:T(8,128)(2,1)S(1)}, u32[]{:S(2)}, u32[]{:S(2)}) collective-permute-start(bf16[1,12,2048]{2,1,0:T(8,128)(2,1)S(1)} %get-tuple-element.39), channel_id=1, source_target_pairs={{0,6},{2,8},{4,10},{6,12},{8,14},{10,16},{12,18},{14,20},{16,22},{... | collective-permute-start | bytes 147464 | tf_op jit(solution)/shard_map/ppermute | solution.py:161
  256.4 5.2 %collective-permute-start.3 = (bf16[1,12,2048]{2,1,0:T(8,128)(2,1)S(1)}, bf16[1,12,2048]{2,1,0:T(8,128)(2,1)S(1)}, u32[]{:S(2)}, u32[]{:S(2)}) collective-permute-start(bf16[1,12,2048]{2,1,0:T(8,128)(2,1)S(1)} %get-tuple-element.38), channel_id=1, source_target_pairs={{0,8},{2,10},{4,12},{6,14},{8,16},{10,18},{12,20},{14,22},{16,24},... | collective-permute-start | bytes 147464 | tf_op jit(solution)/shard_map/ppermute | solution.py:161
  261.5 7.5 %collective-permute-start.4 = (bf16[1,12,2048]{2,1,0:T(8,128)(2,1)S(1)}, bf16[1,12,2048]{2,1,0:T(8,128)(2,1)S(1)}, u32[]{:S(2)}, u32[]{:S(2)}) collective-permute-start(bf16[1,12,2048]{2,1,0:T(8,128)(2,1)S(1)} %get-tuple-element.37), channel_id=1, source_target_pairs={{0,10},{2,12},{4,14},{6,16},{8,18},{10,20},{12,22},{14,24},{16,26}... | collective-permute-start | bytes 147464 | tf_op jit(solution)/shard_map/ppermute | solution.py:161
  269.0 6.1 %collective-permute-start.5 = (bf16[1,12,2048]{2,1,0:T(8,128)(2,1)S(1)}, bf16[1,12,2048]{2,1,0:T(8,128)(2,1)S(1)}, u32[]{:S(2)}, u32[]{:S(2)}) collective-permute-start(bf16[1,12,2048]{2,1,0:T(8,128)(2,1)S(1)} %get-tuple-element.36), channel_id=1, source_target_pairs={{0,12},{2,14},{4,16},{6,18},{8,20},{10,22},{12,24},{14,26},{16,28}... | collective-permute-start | bytes 147464 | tf_op jit(solution)/shard_map/ppermute | solution.py:161
  275.1 6.1 %collective-permute-start.6 = (bf16[1,12,2048]{2,1,0:T(8,128)(2,1)S(1)}, bf16[1,12,2048]{2,1,0:T(8,128)(2,1)S(1)}, u32[]{:S(2)}, u32[]{:S(2)}) collective-permute-start(bf16[1,12,2048]{2,1,0:T(8,128)(2,1)S(1)} %get-tuple-element.35), channel_id=1, source_target_pairs={{0,14},{2,16},{4,18},{6,20},{8,22},{10,24},{12,26},{14,28},{16,30}... | collective-permute-start | bytes 147464 | tf_op jit(solution)/shard_map/ppermute | solution.py:161
  281.2 6.2 %collective-permute-start.7 = (bf16[1,12,2048]{2,1,0:T(8,128)(2,1)S(1)}, bf16[1,12,2048]{2,1,0:T(8,128)(2,1)S(1)}, u32[]{:S(2)}, u32[]{:S(2)}) collective-permute-start(bf16[1,12,2048]{2,1,0:T(8,128)(2,1)S(1)} %get-tuple-element.34), channel_id=1, source_target_pairs={{0,16},{2,18},{4,20},{6,22},{8,24},{10,26},{12,28},{14,30},{16,0},... | collective-permute-start | bytes 147464 | tf_op jit(solution)/shard_map/ppermute | solution.py:161
  287.4 6.1 %collective-permute-start.8 = (bf16[1,12,2048]{2,1,0:T(8,128)(2,1)S(1)}, bf16[1,12,2048]{2,1,0:T(8,128)(2,1)S(1)}, u32[]{:S(2)}, u32[]{:S(2)}) collective-permute-start(bf16[1,12,2048]{2,1,0:T(8,128)(2,1)S(1)} %get-tuple-element.33), channel_id=1, source_target_pairs={{0,18},{2,20},{4,22},{6,24},{8,26},{10,28},{12,30},{14,0},{16,2},{... | collective-permute-start | bytes 147464 | tf_op jit(solution)/shard_map/ppermute | solution.py:161
  293.4 7.4 %collective-permute-start.9 = (bf16[1,12,2048]{2,1,0:T(8,128)(2,1)S(1)}, bf16[1,12,2048]{2,1,0:T(8,128)(2,1)S(1)}, u32[]{:S(2)}, u32[]{:S(2)}) collective-permute-start(bf16[1,12,2048]{2,1,0:T(8,128)(2,1)S(1)} %get-tuple-element.32), channel_id=1, source_target_pairs={{0,20},{2,22},{4,24},{6,26},{8,28},{10,30},{12,0},{14,2},{16,4},{1... | collective-permute-start | bytes 147464 | tf_op jit(solution)/shard_map/ppermute | solution.py:161
  300.8 5.2 %collective-permute-start.10 = (bf16[1,12,2048]{2,1,0:T(8,128)(2,1)S(1)}, bf16[1,12,2048]{2,1,0:T(8,128)(2,1)S(1)}, u32[]{:S(2)}, u32[]{:S(2)}) collective-permute-start(bf16[1,12,2048]{2,1,0:T(8,128)(2,1)S(1)} %get-tuple-element.31), channel_id=1, source_target_pairs={{0,22},{2,24},{4,26},{6,28},{8,30},{10,0},{12,2},{14,4},{16,6},{18... | collective-permute-start | bytes 147464 | tf_op jit(solution)/shard_map/ppermute | solution.py:161
  321.2 32.3 %copy-start.11 = (s32[96]{0:T(128)S(1)}, s32[96]{0:T(128)}, u32[]{:S(2)}) copy-start(s32[96]{0:T(128)} %copy-done.10) | copy-start | bytes 1156
  321.2 32.5 %copy-start.7 = (s32[32,3]{0,1:T(4,128)S(1)}, s32[32,3]{0,1:T(4,128)}, u32[]{:S(2)}) copy-start(s32[32,3]{0,1:T(4,128)} %param.40) | copy-start | bytes 1156
  321.2 60.3 %copy-start.8 = (f32[32,3]{0,1:T(4,128)S(1)}, f32[32,3]{0,1:T(4,128)}, u32[]{:S(2)}) copy-start(f32[32,3]{0,1:T(4,128)} %param.41) | copy-start | bytes 1156
  346.4 36.6 %copy-start.3 = (bf16[32,2048]{1,0:T(8,128)(2,1)S(1)}, bf16[32,2048]{1,0:T(8,128)(2,1)}, u32[]{:S(2)}) copy-start(bf16[32,2048]{1,0:T(8,128)(2,1)} %all-reduce.3.cloned.1.call-done) | copy-start | bytes 393220
  346.4 33.0 %all-to-all-start.1 = ((bf16[16,12,2048]{2,1,0:T(8,128)(2,1)}), bf16[16,12,2048]{2,1,0:T(8,128)(2,1)}, u32[]{:S(2)}, u32[]{:S(2)}) async-start(bf16[16,12,2048]{2,1,0:T(8,128)(2,1)} %copy.65), calls=%async_computation.2 | async-start | bytes 2097152 | tf_op jit(solution)/shard_map/all_to_all | solution.py:182
Sparse Core Ops, SparseCore 0:
  25.9 127.1 reduce-scatter.1
  155.8 49.9 all-gather.1
  208.6 17.9 all-reduce.2
  321.3 22.4 all-reduce.4
